TPU v7x, 32 devices: a whole 2x2x4 slice. The times are simulated.
32 devices in a mesh: ep: 16 (over z, y, x), tp: 2 (over core).
Axes of the slice: x: 2, y: 2, z: 4, core: 2. Of those that a mesh axis runs over, the one named last changes fastest.
Arguments:
- tokens: bfloat16 [384, 2048], P('ep'), may hold values from -6 to 6
- attn_gain: float32 [2048], replicated, may hold values from 0.1 to 1.9
- w_query: bfloat16 [2048, 1024], P(None, 'tp'), may hold values from -0.125 to 0.125
- w_key: bfloat16 [2048, 1024], P(None, 'tp'), may hold values from -0.125 to 0.125
- w_value: bfloat16 [2048, 1024], P(None, 'tp'), may hold values from -0.125 to 0.125
- w_zgate: bfloat16 [2048, 1024], P(None, 'tp'), may hold values from -0.125 to 0.125
- w_decay: bfloat16 [2048, 8], P(None, 'tp'), may hold values from -0.125 to 0.125
- w_beta: bfloat16 [2048, 8], P(None, 'tp'), may hold values from -0.125 to 0.125
- decay_rate: float32 [8], P('tp'), may hold values from 0.05 to 2
- decay_bias: float32 [8], P('tp'), may hold values from -3 to 3
- state: float32 [384, 8, 128, 128], P('ep', 'tp'), may hold values from -2 to 2
- out_gain: float32 [128], replicated, may hold values from 0.1 to 1.9
- w_out: bfloat16 [1024, 2048], P('tp'), may hold values from -0.1875 to 0.1875
- ffn_gain: float32 [2048], replicated, may hold values from 0.1 to 1.9
- expert_gate: bfloat16 [16, 2048, 512], P('ep', None, 'tp'), may hold values from -0.125 to 0.125
- expert_up: bfloat16 [16, 2048, 512], P('ep', None, 'tp'), may hold values from -0.125 to 0.125
- expert_down: bfloat16 [16, 512, 2048], P('ep', 'tp'), may hold values from -0.25 to 0.25
- routes: int32 [384, 2], P('ep'), may hold values from 0 to 15, all different within a row; in each aligned block of 24 rows (0 to 23, 24 to 47, ...) at most 6 rows name the same one
- route_weight: float32 [384, 2], P('ep'), may hold values from 0.2 to 1
Outputs:
- layer_out: bfloat16 [384, 2048], P('ep', 'tp')
- new_state: float32 [384, 8, 128, 128], P('ep', 'tp')
Inputs may be any that keep to these rules, and one draw needn't show every extreme that they name: `routes`: the 2 entries of a row differ. Among the rows of one index of ep (aligned blocks of 24 rows) no expert is named more than 6 times, a bound that some block reaches.
All inputs are finite; a program needn't handle non-finite values.
Results may differ from a plain program's by a relative error of at most 0.014.
Values may be sent and summed in bfloat16 or wider, within the bound.
A program may use at most 128 MiB of HBM per device.

v0:
```python
import jax
import jax.numpy as jnp
from jax import lax
from jax.sharding import PartitionSpec as P

EPS = 1e-06


def rms_scale(rows, gain):
    return rows * lax.rsqrt(jnp.mean(rows * rows, axis=-1, keepdims=True) + EPS) * gain


def unit_rows(rows):
    return rows * lax.rsqrt(jnp.sum(rows * rows, axis=-1, keepdims=True) + EPS)


def per_device(
    tokens,
    attn_gain,
    w_query,
    w_key,
    w_value,
    w_zgate,
    w_decay,
    w_beta,
    decay_rate,
    decay_bias,
    state,
    out_gain,
    w_out,
    ffn_gain,
    expert_gate,
    expert_up,
    expert_down,
    routes,
    route_weight,
):
    seqs, width = tokens.shape
    heads = state.shape[1]
    head_dim = state.shape[2]
    top = routes.shape[1]
    resid_in = tokens.astype(jnp.float32)
    normed = rms_scale(resid_in, attn_gain).astype(jnp.bfloat16)

    def project(weight):
        return jnp.dot(normed, weight, preferred_element_type=jnp.float32).astype(jnp.bfloat16)

    def heads_of(raw):
        return raw.reshape(seqs, heads, head_dim).astype(jnp.float32)

    query = unit_rows(jax.nn.silu(heads_of(project(w_query)))) * head_dim ** (-0.5)
    key = unit_rows(jax.nn.silu(heads_of(project(w_key))))
    value = jax.nn.silu(heads_of(project(w_value)))
    zmul = jax.nn.silu(heads_of(project(w_zgate)))
    fade = jnp.exp(-decay_rate * jax.nn.softplus(project(w_decay).astype(jnp.float32) + decay_bias))
    beta = jax.nn.sigmoid(project(w_beta).astype(jnp.float32))
    predicted = jnp.einsum("shkv,shk->shv", state, key, precision=lax.Precision.HIGHEST)
    written = beta[..., None] * (value - fade[..., None] * predicted)
    new_state = fade[..., None, None] * state + key[..., :, None] * written[..., None, :]
    read = jnp.einsum("shkv,shk->shv", new_state, query, precision=lax.Precision.HIGHEST)
    heads_out = (
        (rms_scale(read, out_gain) * zmul).astype(jnp.bfloat16).reshape(seqs, heads * head_dim)
    )
    partial_value = jnp.dot(heads_out, w_out, preferred_element_type=jnp.float32)
    mixed = lax.psum(partial_value.astype(jnp.bfloat16), "tp").astype(jnp.float32)
    resid = resid_in + mixed
    moe_in = rms_scale(resid, ffn_gain).astype(jnp.bfloat16)
    experts = lax.axis_size("ep")
    cap = max(2, 2 * seqs * top // experts)
    flat_routes = routes.reshape(-1)
    onehot = (flat_routes[:, None] == jnp.arange(experts, dtype=jnp.int32)[None, :]).astype(
        jnp.int32
    )
    before = jnp.cumsum(onehot, axis=0) - onehot
    slot = jnp.sum(before * onehot, axis=1)
    place = flat_routes * cap + slot
    pick = (place[:, None] == jnp.arange(experts * cap, dtype=jnp.int32)[None, :]).astype(
        jnp.bfloat16
    )
    columns = width // lax.axis_size("tp")
    own_part = lax.dynamic_slice_in_dim(moe_in, lax.axis_index("tp") * columns, columns, 1)
    spread = jnp.repeat(own_part, top, axis=0)
    outgoing = jnp.dot(pick.T, spread, preferred_element_type=jnp.float32).astype(jnp.bfloat16)
    outgoing = outgoing.reshape(experts, 1, cap, columns)
    arrived = lax.all_gather(
        lax.all_to_all(outgoing, "ep", split_axis=0, concat_axis=1, tiled=True),
        "tp",
        axis=3,
        tiled=True,
    )
    flat_rows = arrived.reshape(-1, arrived.shape[-1])
    gate = jnp.dot(flat_rows, expert_gate[0], preferred_element_type=jnp.float32)
    up = jnp.dot(flat_rows, expert_up[0], preferred_element_type=jnp.float32)
    hidden = (jax.nn.silu(gate) * up).astype(jnp.bfloat16)
    term = jnp.dot(hidden, expert_down[0], preferred_element_type=jnp.float32)
    terms = term.reshape(arrived.shape[:-1] + (term.shape[-1],))
    summed = lax.psum_scatter(terms.astype(jnp.bfloat16), "tp", scatter_dimension=3, tiled=True)
    returned = lax.all_to_all(summed, "ep", split_axis=1, concat_axis=0, tiled=True)
    returned = returned.reshape(experts * cap, columns)
    per_route = jnp.dot(pick, returned, preferred_element_type=jnp.float32).reshape(
        seqs, top, columns
    )
    combined = jnp.sum(per_route * route_weight[..., None], axis=1)
    own_resid = lax.dynamic_slice_in_dim(resid, lax.axis_index("tp") * columns, columns, 1)
    layer_out = (own_resid + combined).astype(jnp.bfloat16)
    return (layer_out, new_state)


def solution(mesh):
    in_specs = (
        P("ep", None),
        P(),
        P(None, "tp"),
        P(None, "tp"),
        P(None, "tp"),
        P(None, "tp"),
        P(None, "tp"),
        P(None, "tp"),
        P("tp"),
        P("tp"),
        P("ep", "tp", None, None),
        P(),
        P("tp", None),
        P(),
        P("ep", None, "tp"),
        P("ep", None, "tp"),
        P("ep", "tp", None),
        P("ep", None),
        P("ep", None),
    )
    out_specs = (P("ep", "tp"), P("ep", "tp", None, None))
    return jax.shard_map(
        per_device, mesh=mesh, in_specs=in_specs, out_specs=out_specs, check_vma=False
    )
```

profile of v0, /device:TPU:0, one launch (start us, length us, event | category | flops | bytes accessed | tf_op | source)
XLA Modules:
  0.0 115.3 jit_solution(10898759450930380615)
XLA Ops:
  7.3 1.2 %fusion.18 = f32[24]{0:T(128)S(1)} fusion(bf16[24,2048]{1,0:T(8,128)(2,1)} %param.19), kind=kLoop, calls=%fused_computation.33 | loop fusion | flops 147432 | bytes 98400 | tf_op jit(solution)/shard_map/reduce_sum | solution.py:10
  8.5 2.1 %fusion.6 = f32[24,512]{1,0:T(8,128)S(1)} fusion(bf16[2048,512]{1,0:T(8,128)(2,1)} %param.22, bf16[24,2048]{1,0:T(8,128)(2,1)} %param.19, f32[2048]{0:T(1024)} %param.20, f32[24]{0:T(128)S(1)} %add_rsqrt_fusion.4), kind=kOutput, calls=%fused_computation.16 | convolution fusion | flops 50552832 | bytes 2252896 | tf_op jit(solution)/shard_map/dot_general | solution.py:46
  10.6 0.1 multiply_reduce_fusion.3
  10.9 0.2 fusion.34
  11.2 2.0 %fusion.5 = f32[24,512]{1,0:T(8,128)S(1)} fusion(bf16[2048,512]{1,0:T(8,128)(2,1)} %param.23, bf16[24,2048]{1,0:T(8,128)(2,1)S(1)} %copy-done.2, f32[2048]{0:T(1024)S(1)} %copy-done.5, f32[24]{0:T(128)S(1)} %add_rsqrt_fusion.4), kind=kOutput, calls=%fused_computation.14 | convolution fusion | flops 50552832 | bytes 2252896 | tf_op jit(solution)/shard_map/dot_general | solution.py:46
  13.3 0.2 fusion.13
  13.6 8.1 %fusion.41 = f32[24,4,1,128]{3,2,1,0:T(1,128)S(1)} fusion(f32[24,4,128,1]{2,3,1,0:T(1,128)S(1)} %bitcast.48, f32[24,4,128,128]{3,2,1,0:T(8,128)} %param.29), kind=kOutput, calls=%fused_computation.73 | convolution fusion | flops 18874368 | bytes 6389760 | tf_op jit(solution)/shard_map/shkv,shk->shv/dot_general | solution.py:57
  21.7 0.1 fusion.24
  21.8 3.9 %multiply_add_fusion = f32[24,4,128,128]{3,2,1,0:T(8,128)} fusion(f32[24,4,128,128]{3,2,1,0:T(8,128)S(1)} %copy-done.1, f32[24,4,128]{2,1,0:T(4,128)S(1)} %fusion.24, f32[24,4,128]{2,1,0:T(4,128)S(1)} %broadcast_multiply_fusion, f32[24,4]{1,0:T(8,128)S(1)} %copy.48), kind=kLoop, calls=%fused_computation | loop fusion | flops 4718592 | bytes 12681600 | tf_op jit(solution)/shard_map/add | solution.py:59
  25.7 0.4 fusion.4
  26.2 0.1 multiply_reduce_fusion.2
  26.4 7.5 %fusion.42 = f32[24,4,1,128]{3,2,1,0:T(1,128)S(1)} fusion(f32[24,4,128,128]{3,2,1,0:T(8,128)} %multiply_add_fusion, f32[24,4,128,1]{2,3,1,0:T(1,128)S(1)} %bitcast.51), kind=kOutput, calls=%fused_computation.74 | convolution fusion | flops 18874368 | bytes 6389760 | tf_op jit(solution)/shard_map/shkv,shk->shv/dot_general | solution.py:60
  33.9 0.1 multiply_reduce_fusion.1
  34.1 0.4 fusion.3
  34.6 0.1 fusion.25
  34.7 1.0 convolution_convert_fusion.1
  36.2 0.2 select_reduce_fusion
  36.4 20.1 %all-reduce.2.cloned.1.call-done = bf16[24,2048]{1,0:T(8,128)(2,1)} async-done(((bf16[24,2048]{1,0:T(8,128)(2,1)}), bf16[24,2048]{1,0:T(8,128)(2,1)}) %all-reduce.2.cloned.1.call-update) | async-done | bytes 98320 | tf_op jit(solution)/shard_map/psum | solution.py:65
  56.5 1.0 multiply_reduce_fusion
  57.7 0.3 convolution_convert_fusion.2
  58.1 16.9 %all_to_all.21 = bf16[16,1,6,1024]{3,2,1,0:T(8,128)(2,1)S(1)} all-to-all(bf16[16,1,6,1024]{3,2,1,0:T(8,128)(2,1)S(1)} %bitcast.47), channel_id=1, replica_groups=mesh['ep'=16,'tp'=2] {'ep'}, dimensions={0} | all-to-all | bytes 393216 | tf_op jit(solution)/shard_map/all_to_all | solution.py:86
  75.0 2.2 %all-gather = bf16[16,1,6,2048]{3,2,1,0:T(8,128)(2,1)S(1)} all-gather(bf16[16,1,6,1024]{3,2,1,0:T(8,128)(2,1)S(1)} %all_to_all.21), channel_id=2, replica_groups=mesh['ep'=16,'tp'=2] {'tp'}, dimensions={3}, use_global_device_ids=true | all-gather | bytes 589824 | tf_op jit(solution)/shard_map/all_gather | solution.py:85
  77.2 0.1 reshape.137
  77.3 1.5 %fusion.16 = f32[96,256]{1,0:T(8,128)S(1)} fusion(bf16[96,2048]{1,0:T(8,128)(2,1)S(1)} %reshape.137, bf16[1,2048,256]{2,1,0:T(8,128)(2,1)} %param.33), kind=kOutput, calls=%fused_computation.28 | convolution fusion | flops 100663296 | bytes 1540096 | tf_op jit(solution)/shard_map/dot_general | solution.py:92
  78.9 1.5 %fusion.2 = bf16[96,256]{1,0:T(8,128)(2,1)S(1)} fusion(bf16[96,2048]{1,0:T(8,128)(2,1)S(1)} %reshape.137, bf16[1,2048,256]{2,1,0:T(8,128)(2,1)} %param.34, f32[96,256]{1,0:T(8,128)S(1)} %fusion.16), kind=kOutput, calls=%fused_computation.8 | convolution fusion | flops 100810752 | bytes 1589248 | tf_op jit(solution)/shard_map/dot_general | solution.py:93
  80.5 2.3 %fusion = bf16[1,16,6,2048]{3,1,2,0:T(8,128)(2,1)} fusion(bf16[1,256,2048]{2,1,0:T(8,128)(2,1)} %param.35, bf16[16,6,256]{2,1,0:T(8,128)(2,1)S(1)} %dot_general.56), kind=kOutput, calls=%fused_computation.2 | convolution fusion | flops 100859904 | bytes 1490944 | tf_op jit(solution)/shard_map/dot_general | solution.py:95
  82.8 5.9 %reduce-scatter.2.cloned.1.call-done = bf16[1,16,6,1024]{3,1,2,0:T(8,128)(2,1)} async-done(((bf16[1,16,6,2048]{3,1,2,0:T(8,128)(2,1)}), bf16[1,16,6,1024]{3,1,2,0:T(8,128)(2,1)}) %reduce-scatter.2.cloned.1.call-update) | async-done | bytes 196624 | tf_op jit(solution)/shard_map/reduce_scatter | solution.py:97
  88.6 1.7 %copy.55 = bf16[1,16,6,1024]{3,2,0,1:T(8,128)(2,1)} copy(bf16[1,16,6,1024]{3,1,2,0:T(8,128)(2,1)} %reduce-scatter.2.cloned.1.call-done) | data formatting | bytes 393216 | tf_op jit(solution)/shard_map/reduce_scatter | solution.py:97
  90.4 6.7 %all-to-all-start.1 = ((bf16[1,16,6,1024]{3,2,0,1:T(8,128)(2,1)}), bf16[1,16,6,1024]{3,2,0,1:T(8,128)(2,1)S(1)}, u32[]{:S(2)}, u32[]{:S(2)}) async-start(bf16[1,16,6,1024]{3,2,0,1:T(8,128)(2,1)} %copy.55), calls=%async_computation.2 | async-start | bytes 524288 | tf_op jit(solution)/shard_map/all_to_all | solution.py:98
  97.3 10.2 %all-to-all-done.1 = bf16[1,16,6,1024]{3,2,0,1:T(8,128)(2,1)S(1)} async-done(((bf16[1,16,6,1024]{3,2,0,1:T(8,128)(2,1)}), bf16[1,16,6,1024]{3,2,0,1:T(8,128)(2,1)S(1)}, u32[]{:S(2)}, u32[]{:S(2)}) %all-to-all-start.1) | async-done | bytes 196640 | tf_op jit(solution)/shard_map/all_to_all | solution.py:98
  107.6 0.2 fusion.1
  107.8 0.6 add_convert_fusion
  (61 shorter events, 1.6 us)
Async XLA Ops:
  7.2 27.5 %copy-start = (bf16[512,2048]{1,0:T(8,128)(2,1)S(1)}, bf16[512,2048]{1,0:T(8,128)(2,1)}, u32[]{:S(2)}) copy-start(bf16[512,2048]{1,0:T(8,128)(2,1)} %param.31) | copy-start | bytes 6291460
  7.2 3.7 %copy-start.2 = (bf16[24,2048]{1,0:T(8,128)(2,1)S(1)}, bf16[24,2048]{1,0:T(8,128)(2,1)}, u32[]{:S(2)}) copy-start(bf16[24,2048]{1,0:T(8,128)(2,1)} %param.19) | copy-start | bytes 294916
  7.2 3.7 %copy-start.5 = (f32[2048]{0:T(1024)S(1)}, f32[2048]{0:T(1024)}, u32[]{:S(2)}) copy-start(f32[2048]{0:T(1024)} %param.20) | copy-start | bytes 24580
  7.2 3.6 %copy-start.12 = (f32[4]{0:T(128)S(1)}, f32[4]{0:T(128)}, u32[]{:S(2)}) copy-start(f32[4]{0:T(128)} %param.27) | copy-start | bytes 52
  7.2 3.7 %copy-start.10 = (bf16[2048,4]{0,1:T(4,128)(2,1)S(1)}, bf16[2048,4]{0,1:T(4,128)(2,1)}, u32[]{:S(2)}) copy-start(bf16[2048,4]{0,1:T(4,128)(2,1)} %param.25) | copy-start | bytes 49156
  7.2 3.7 %copy-start.13 = (f32[4]{0:T(128)S(1)}, f32[4]{0:T(128)}, u32[]{:S(2)}) copy-start(f32[4]{0:T(128)} %param.28) | copy-start | bytes 52
  7.2 49.2 %all-reduce.2.cloned.1.call-start = ((), (), s32[]{:S(2)}) async-start(), calls=%async_computation.3 | async-start | bytes 196608 | tf_op jit(solution)/shard_map/psum | solution.py:65
  8.4 4.8 %copy-start.11 = (bf16[2048,4]{0,1:T(4,128)(2,1)S(1)}, bf16[2048,4]{0,1:T(4,128)(2,1)}, u32[]{:S(2)}) copy-start(bf16[2048,4]{0,1:T(4,128)(2,1)} %param.26) | copy-start | bytes 49156
  13.6 8.2 %copy-start.1 = (f32[24,4,128,128]{3,2,1,0:T(8,128)S(1)}, f32[24,4,128,128]{3,2,1,0:T(8,128)}, u32[]{:S(2)}) copy-start(f32[24,4,128,128]{3,2,1,0:T(8,128)} %param.29) | copy-start | bytes 18874372
  21.8 3.9 %copy-start.3 = (bf16[2048,512]{1,0:T(8,128)(2,1)S(1)}, bf16[2048,512]{1,0:T(8,128)(2,1)}, u32[]{:S(2)}) copy-start(bf16[2048,512]{1,0:T(8,128)(2,1)} %param.21) | copy-start | bytes 6291460
  26.4 7.7 %copy-start.4 = (bf16[2048,512]{1,0:T(8,128)(2,1)S(1)}, bf16[2048,512]{1,0:T(8,128)(2,1)}, u32[]{:S(2)}) copy-start(bf16[2048,512]{1,0:T(8,128)(2,1)} %param.24) | copy-start | bytes 6291460
  33.9 0.7 copy-start.9
  34.1 1.7 %copy-start.6 = (s32[24,2]{0,1:T(2,128)S(1)}, s32[24,2]{0,1:T(2,128)}, u32[]{:S(2)}) copy-start(s32[24,2]{0,1:T(2,128)} %param.36) | copy-start | bytes 580
  34.1 2.3 %copy-start.7 = (f32[2048]{0:T(1024)S(1)}, f32[2048]{0:T(1024)}, u32[]{:S(2)}) copy-start(f32[2048]{0:T(1024)} %param.32) | copy-start | bytes 24580
  35.8 52.9 %reduce-scatter.2.cloned.1.call-start = ((), (), s32[]{:S(2)}) async-start(), calls=%async_computation.4 | async-start | bytes 589824 | tf_op jit(solution)/shard_map/reduce_scatter | solution.py:97
  80.4 27.2 %copy-start.8 = (f32[24,2]{0,1:T(2,128)S(1)}, f32[24,2]{0,1:T(2,128)}, u32[]{:S(2)}) copy-start(f32[24,2]{0,1:T(2,128)} %param.37) | copy-start | bytes 580
  90.4 17.1 %all-to-all-start.1 = ((bf16[1,16,6,1024]{3,2,0,1:T(8,128)(2,1)}), bf16[1,16,6,1024]{3,2,0,1:T(8,128)(2,1)S(1)}, u32[]{:S(2)}, u32[]{:S(2)}) async-start(bf16[1,16,6,1024]{3,2,0,1:T(8,128)(2,1)} %copy.55), calls=%async_computation.2 | async-start | bytes 524288 | tf_op jit(solution)/shard_map/all_to_all | solution.py:98
Sparse Core Ops, SparseCore 0:
  35.9 20.5 all-reduce.1
  82.9 5.7 reduce-scatter.1
where the time goes:
time: 116 us; the launch traced here: 115 us
  waiting for transfers between devices  36.2 us (31%)
  matrix products  28 us (24%)
  blocking collectives  19.1 us (16%)
  between operations  14.4 us (12%)
  other arithmetic  7.91 us (7%)
  starting transfers between devices  6.81 us (6%)
  local copies, waits for them, and re-layouts  2.86 us (2%)
    psum x1, waiting for transfers between devices, per_device(): lax.psum(partial_value.astype(jnp.bfloat16), 'tp').astype(jnp.float32)  20.1 us
    all_to_all x1, blocking collectives, per_device(): lax.all_to_all(outgoing, 'ep', split_axis=0, concat_axis=1, tiled=True)  16.9 us
    all_to_all x1, waiting for transfers between devices, per_device(): lax.all_to_all(summed, 'ep', split_axis=1, concat_axis=0, tiled=True)  10.2 us
    dot_general x1, matrix products, per_device(): jnp.einsum('shkv,shk->shv', state, key, precision=lax.Precision.HIGHEST)  8.09 us
    dot_general x1, matrix products, per_device(): jnp.einsum('shkv,shk->shv', new_state, query, precision=lax.Precision.HIG...  7.54 us
    all_to_all x1, starting transfers between devices, per_device(): lax.all_to_all(summed, 'ep', split_axis=1, concat_axis=0, tiled=True)  6.73 us
    reduce_scatter x1, waiting for transfers between devices, per_device(): lax.psum_scatter(terms.astype(jnp.bfloat16), 'tp', scatter_dimension=3, t...  5.89 us
    dot_general x6, matrix products, project(): jnp.dot(normed, weight, preferred_element_type=jnp.float32)  5.45 us
  transfers between devices with their start and end apart: 3, of which 3 were waited for; matrix products, arithmetic and copies ran while one was open for 1% of the time, Pallas kernels for 0%

commit v1 on v0

--- a/solution.py
+++ b/solution.py
@@ -95,7 +95,10 @@
     term = jnp.dot(hidden, expert_down[0], preferred_element_type=jnp.float32)
     terms = term.reshape(arrived.shape[:-1] + (term.shape[-1],))
     summed = lax.psum_scatter(terms.astype(jnp.bfloat16), "tp", scatter_dimension=3, tiled=True)
-    returned = lax.all_to_all(summed, "ep", split_axis=1, concat_axis=0, tiled=True)
+    returned = jnp.concatenate(
+        lax.all_to_all(jnp.stack(jnp.split(summed, lax.axis_size("ep"), axis=1)), "ep", 0, 0),
+        axis=0,
+    )
     returned = returned.reshape(experts * cap, columns)
     per_route = jnp.dot(pick, returned, preferred_element_type=jnp.float32).reshape(
         seqs, top, columns

time: 116 us -> 126 us (1.086)
  local copies, waits for them, and re-layouts: 2.86 us -> 13.1 us
    unnamed x29 -> x44, local copies, waits for them, and re-layouts: 0.2 us -> 9.3 us
    split x0 -> x1, local copies, waits for them, and re-layouts: none -> 2.23 us  [per_device(): jnp.split(summed, lax.axis_size('ep'), axis=1)]
    reduce_scatter x1 -> x0, local copies, waits for them, and re-layouts: 1.73 us -> none  [per_device(): lax.psum_scatter(terms.astype(jnp.bfloat16), 'tp', scatter_dimension=3, t...]
where the time goes in v1:
time: 126 us
  waiting for transfers between devices  36.2 us (29%)
  matrix products  28 us (22%)
  blocking collectives  19.1 us (15%)
  between operations  14.5 us (12%)
  local copies, waits for them, and re-layouts  13.1 us (10%)
  other arithmetic  7.91 us (6%)
  starting transfers between devices  6.81 us (5%)
    psum x1, waiting for transfers between devices, per_device(): lax.psum(partial_value.astype(jnp.bfloat16), 'tp').astype(jnp.float32)  20.1 us
    all_to_all x1, blocking collectives, per_device(): lax.all_to_all(outgoing, 'ep', split_axis=0, concat_axis=1, tiled=True)  16.9 us
    all_to_all x1, waiting for transfers between devices, per_device(): lax.all_to_all(jnp.stack(jnp.split(summed, lax.axis_size('ep'), axis=1)),...  10.2 us
    unnamed x44, local copies, waits for them, and re-layouts  9.3 us
    dot_general x1, matrix products, per_device(): jnp.einsum('shkv,shk->shv', state, key, precision=lax.Precision.HIGHEST)  8.09 us
    dot_general x1, matrix products, per_device(): jnp.einsum('shkv,shk->shv', new_state, query, precision=lax.Precision.HIG...  7.54 us
    all_to_all x1, starting transfers between devices, per_device(): lax.all_to_all(jnp.stack(jnp.split(summed, lax.axis_size('ep'), axis=1)),...  6.73 us
    reduce_scatter x1, waiting for transfers between devices, per_device(): lax.psum_scatter(terms.astype(jnp.bfloat16), 'tp', scatter_dimension=3, t...  5.89 us
  transfers between devices with their start and end apart: 3, of which 3 were waited for; matrix products, arithmetic and copies ran while one was open for 1% of the time, Pallas kernels for 0%

profile of v1, /device:TPU:0, one launch (start us, length us, event | category | flops | bytes accessed | tf_op | source)
XLA Modules:
  0.0 125.5 jit_solution(14143242713647247710)
XLA Ops:
  7.3 1.2 fusion.18
  8.5 2.1 %fusion.6 = f32[24,512]{1,0:T(8,128)S(1)} fusion(bf16[2048,512]{1,0:T(8,128)(2,1)} %param.22, bf16[24,2048]{1,0:T(8,128)(2,1)} %param.19, f32[2048]{0:T(1024)} %param.20, f32[24]{0:T(128)S(1)} %add_rsqrt_fusion.4), kind=kOutput, calls=%fused_computation.16 | convolution fusion | flops 50552832 | bytes 2252896 | tf_op jit(solution)/shard_map/dot_general | solution.py:46
  11.2 2.0 %fusion.5 = f32[24,512]{1,0:T(8,128)S(1)} fusion(bf16[2048,512]{1,0:T(8,128)(2,1)} %param.23, bf16[24,2048]{1,0:T(8,128)(2,1)S(1)} %copy-done.2, f32[2048]{0:T(1024)S(1)} %copy-done.5, f32[24]{0:T(128)S(1)} %add_rsqrt_fusion.4), kind=kOutput, calls=%fused_computation.14 | convolution fusion | flops 50552832 | bytes 2252896 | tf_op jit(solution)/shard_map/dot_general | solution.py:46
  13.6 8.1 %fusion.42 = f32[24,4,1,128]{3,2,1,0:T(1,128)S(1)} fusion(f32[24,4,128,1]{2,3,1,0:T(1,128)S(1)} %bitcast.78, f32[24,4,128,128]{3,2,1,0:T(8,128)} %param.29), kind=kOutput, calls=%fused_computation.90 | convolution fusion | flops 18874368 | bytes 6389760 | tf_op jit(solution)/shard_map/shkv,shk->shv/dot_general | solution.py:57
  21.8 3.9 %multiply_add_fusion = f32[24,4,128,128]{3,2,1,0:T(8,128)} fusion(f32[24,4,128,128]{3,2,1,0:T(8,128)S(1)} %copy-done.1, f32[24,4,128]{2,1,0:T(4,128)S(1)} %fusion.24, f32[24,4,128]{2,1,0:T(4,128)S(1)} %broadcast_multiply_fusion, f32[24,4]{1,0:T(8,128)S(1)} %copy.286), kind=kLoop, calls=%fused_computation | loop fusion | flops 4718592 | bytes 12681600 | tf_op jit(solution)/shard_map/add | solution.py:59
  26.4 7.5 %fusion.43 = f32[24,4,1,128]{3,2,1,0:T(1,128)S(1)} fusion(f32[24,4,128,128]{3,2,1,0:T(8,128)} %multiply_add_fusion, f32[24,4,128,1]{2,3,1,0:T(1,128)S(1)} %bitcast.81), kind=kOutput, calls=%fused_computation.91 | convolution fusion | flops 18874368 | bytes 6389760 | tf_op jit(solution)/shard_map/shkv,shk->shv/dot_general | solution.py:60
  34.7 1.0 convolution_convert_fusion.1
  36.4 20.1 %all-reduce.2.cloned.1.call-done = bf16[24,2048]{1,0:T(8,128)(2,1)} async-done(((bf16[24,2048]{1,0:T(8,128)(2,1)}), bf16[24,2048]{1,0:T(8,128)(2,1)}) %all-reduce.2.cloned.1.call-update) | async-done | bytes 98320 | tf_op jit(solution)/shard_map/psum | solution.py:65
  56.5 1.0 multiply_reduce_fusion
  58.1 16.9 %all_to_all.17 = bf16[16,1,6,1024]{3,2,1,0:T(8,128)(2,1)S(1)} all-to-all(bf16[16,1,6,1024]{3,2,1,0:T(8,128)(2,1)S(1)} %bitcast.77), channel_id=1, replica_groups=mesh['ep'=16,'tp'=2] {'ep'}, dimensions={0} | all-to-all | bytes 393216 | tf_op jit(solution)/shard_map/all_to_all | solution.py:86
  75.0 2.2 %all-gather = bf16[16,1,6,2048]{3,2,1,0:T(8,128)(2,1)S(1)} all-gather(bf16[16,1,6,1024]{3,2,1,0:T(8,128)(2,1)S(1)} %all_to_all.17), channel_id=2, replica_groups=mesh['ep'=16,'tp'=2] {'tp'}, dimensions={3}, use_global_device_ids=true | all-gather | bytes 589824 | tf_op jit(solution)/shard_map/all_gather | solution.py:85
  77.3 1.5 %fusion.16 = f32[96,256]{1,0:T(8,128)S(1)} fusion(bf16[96,2048]{1,0:T(8,128)(2,1)S(1)} %reshape.130, bf16[1,2048,256]{2,1,0:T(8,128)(2,1)} %param.33), kind=kOutput, calls=%fused_computation.28 | convolution fusion | flops 100663296 | bytes 1540096 | tf_op jit(solution)/shard_map/dot_general | solution.py:92
  78.9 1.5 %fusion.2 = bf16[96,256]{1,0:T(8,128)(2,1)S(1)} fusion(bf16[96,2048]{1,0:T(8,128)(2,1)S(1)} %reshape.130, bf16[1,2048,256]{2,1,0:T(8,128)(2,1)} %param.34, f32[96,256]{1,0:T(8,128)S(1)} %fusion.16), kind=kOutput, calls=%fused_computation.8 | convolution fusion | flops 100810752 | bytes 1589248 | tf_op jit(solution)/shard_map/dot_general | solution.py:93
  80.5 2.3 %fusion = bf16[1,16,6,2048]{3,1,2,0:T(8,128)(2,1)} fusion(bf16[1,256,2048]{2,1,0:T(8,128)(2,1)} %param.35, bf16[16,6,256]{2,1,0:T(8,128)(2,1)S(1)} %dot_general.56), kind=kOutput, calls=%fused_computation.2 | convolution fusion | flops 100859904 | bytes 1490944 | tf_op jit(solution)/shard_map/dot_general | solution.py:95
  82.8 5.9 %reduce-scatter.2.cloned.1.call-done = bf16[1,16,6,1024]{3,1,2,0:T(8,128)(2,1)} async-done(((bf16[1,16,6,2048]{3,1,2,0:T(8,128)(2,1)}), bf16[1,16,6,1024]{3,1,2,0:T(8,128)(2,1)}) %reduce-scatter.2.cloned.1.call-update) | async-done | bytes 196624 | tf_op jit(solution)/shard_map/reduce_scatter | solution.py:97
  88.7 2.2 %fusion.41 = (bf16[1,1,6,1024]{3,1,2,0:T(2,128)(2,1)S(1)}, bf16[1,1,6,1024]{3,1,2,0:T(2,128)(2,1)S(1)}, bf16[1,1,6,1024]{3,1,2,0:T(2,128)(2,1)S(1)}, bf16[1,1,6,...) fusion(bf16[1,16,6,1024]{3,1,2,0:T(8,128)(2,1)} %reduce-scatter, ...), kind=kLoop, calls=%fused_computation.89 | loop fusion | bytes 393216 | tf_op jit(solution)/shard_map/split | solution.py:99
  91.5 0.6 constant_dynamic-update-slice_fusion.14
  92.1 0.6 constant_dynamic-update-slice_fusion.13
  92.7 0.6 constant_dynamic-update-slice_fusion.12
  93.3 0.6 constant_dynamic-update-slice_fusion.11
  93.9 0.6 constant_dynamic-update-slice_fusion.10
  94.5 0.6 constant_dynamic-update-slice_fusion.9
  95.1 0.6 constant_dynamic-update-slice_fusion.8
  95.7 0.6 constant_dynamic-update-slice_fusion.7
  97.0 0.6 constant_dynamic-update-slice_fusion.5
  97.6 0.6 constant_dynamic-update-slice_fusion.4
  98.2 0.6 constant_dynamic-update-slice_fusion.3
  99.4 0.6 constant_dynamic-update-slice_fusion.1
  100.0 0.6 constant_dynamic-update-slice_fusion
  100.6 6.7 %all-to-all-start.1 = ((bf16[16,1,1,6,1024]{4,3,2,1,0:T(8,128)(2,1)}), bf16[16,1,1,6,1024]{4,3,2,1,0:T(8,128)(2,1)S(1)}, u32[]{:S(2)}, u32[]{:S(2)}) async-start(bf16[16,1,1,6,1024]{4,3,2,1,0:T(8,128)(2,1)} %constant_dynamic-update-slice_fusion), calls=%async_computation.2 | async-start | bytes 524288 | tf_op jit(solution)/shard_map/all_to_all | solution.py:99
  107.5 10.2 %all-to-all-done.1 = bf16[16,1,1,6,1024]{4,3,2,1,0:T(8,128)(2,1)S(1)} async-done(((bf16[16,1,1,6,1024]{4,3,2,1,0:T(8,128)(2,1)}), bf16[16,1,1,6,1024]{4,3,2,1,0:T(8,128)(2,1)S(1)}, u32[]{:S(2)}, u32[]{:S(2)}) %all-to-all-start.1) | async-done | bytes 196640 | tf_op jit(solution)/shard_map/all_to_all | solution.py:99
  118.0 0.6 add_convert_fusion
  (77 shorter events, 6.1 us)
Async XLA Ops:
  7.2 27.5 %copy-start = (bf16[512,2048]{1,0:T(8,128)(2,1)S(1)}, bf16[512,2048]{1,0:T(8,128)(2,1)}, u32[]{:S(2)}) copy-start(bf16[512,2048]{1,0:T(8,128)(2,1)} %param.31) | copy-start | bytes 6291460
  7.2 3.7 %copy-start.2 = (bf16[24,2048]{1,0:T(8,128)(2,1)S(1)}, bf16[24,2048]{1,0:T(8,128)(2,1)}, u32[]{:S(2)}) copy-start(bf16[24,2048]{1,0:T(8,128)(2,1)} %param.19) | copy-start | bytes 294916
  7.2 3.7 %copy-start.5 = (f32[2048]{0:T(1024)S(1)}, f32[2048]{0:T(1024)}, u32[]{:S(2)}) copy-start(f32[2048]{0:T(1024)} %param.20) | copy-start | bytes 24580
  7.2 3.6 %copy-start.12 = (f32[4]{0:T(128)S(1)}, f32[4]{0:T(128)}, u32[]{:S(2)}) copy-start(f32[4]{0:T(128)} %param.27) | copy-start | bytes 52
  7.2 3.7 %copy-start.10 = (bf16[2048,4]{0,1:T(4,128)(2,1)S(1)}, bf16[2048,4]{0,1:T(4,128)(2,1)}, u32[]{:S(2)}) copy-start(bf16[2048,4]{0,1:T(4,128)(2,1)} %param.25) | copy-start | bytes 49156
  7.2 3.7 %copy-start.13 = (f32[4]{0:T(128)S(1)}, f32[4]{0:T(128)}, u32[]{:S(2)}) copy-start(f32[4]{0:T(128)} %param.28) | copy-start | bytes 52
  7.2 49.2 %all-reduce.2.cloned.1.call-start = ((), (), s32[]{:S(2)}) async-start(), calls=%async_computation.3 | async-start | bytes 196608 | tf_op jit(solution)/shard_map/psum | solution.py:65
  8.4 4.8 %copy-start.11 = (bf16[2048,4]{0,1:T(4,128)(2,1)S(1)}, bf16[2048,4]{0,1:T(4,128)(2,1)}, u32[]{:S(2)}) copy-start(bf16[2048,4]{0,1:T(4,128)(2,1)} %param.26) | copy-start | bytes 49156
  13.6 8.2 %copy-start.1 = (f32[24,4,128,128]{3,2,1,0:T(8,128)S(1)}, f32[24,4,128,128]{3,2,1,0:T(8,128)}, u32[]{:S(2)}) copy-start(f32[24,4,128,128]{3,2,1,0:T(8,128)} %param.29) | copy-start | bytes 18874372
  21.8 3.9 %copy-start.3 = (bf16[2048,512]{1,0:T(8,128)(2,1)S(1)}, bf16[2048,512]{1,0:T(8,128)(2,1)}, u32[]{:S(2)}) copy-start(bf16[2048,512]{1,0:T(8,128)(2,1)} %param.21) | copy-start | bytes 6291460
  26.4 7.7 %copy-start.4 = (bf16[2048,512]{1,0:T(8,128)(2,1)S(1)}, bf16[2048,512]{1,0:T(8,128)(2,1)}, u32[]{:S(2)}) copy-start(bf16[2048,512]{1,0:T(8,128)(2,1)} %param.24) | copy-start | bytes 6291460
  33.9 0.7 copy-start.9
  34.1 1.7 %copy-start.6 = (s32[24,2]{0,1:T(2,128)S(1)}, s32[24,2]{0,1:T(2,128)}, u32[]{:S(2)}) copy-start(s32[24,2]{0,1:T(2,128)} %param.36) | copy-start | bytes 580
  34.1 2.3 %copy-start.7 = (f32[2048]{0:T(1024)S(1)}, f32[2048]{0:T(1024)}, u32[]{:S(2)}) copy-start(f32[2048]{0:T(1024)} %param.32) | copy-start | bytes 24580
  35.8 52.9 %reduce-scatter.2.cloned.1.call-start = ((), (), s32[]{:S(2)}) async-start(), calls=%async_computation.4 | async-start | bytes 589824 | tf_op jit(solution)/shard_map/reduce_scatter | solution.py:97
  80.4 37.4 %copy-start.8 = (f32[24,2]{0,1:T(2,128)S(1)}, f32[24,2]{0,1:T(2,128)}, u32[]{:S(2)}) copy-start(f32[24,2]{0,1:T(2,128)} %param.37) | copy-start | bytes 580
  100.6 17.1 %all-to-all-start.1 = ((bf16[16,1,1,6,1024]{4,3,2,1,0:T(8,128)(2,1)}), bf16[16,1,1,6,1024]{4,3,2,1,0:T(8,128)(2,1)S(1)}, u32[]{:S(2)}, u32[]{:S(2)}) async-start(bf16[16,1,1,6,1024]{4,3,2,1,0:T(8,128)(2,1)} %constant_dynamic-update-slice_fusion), calls=%async_computation.2 | async-start | bytes 524288 | tf_op jit(solution)/shard_map/all_to_all | solution.py:99
Sparse Core Ops, SparseCore 0:
  35.9 20.5 all-reduce.1
  82.9 5.7 reduce-scatter.1
